TPU v7x, 512 devices: a whole 4x4x16 slice. The times are simulated.
512 devices in a mesh: ep: 32 (over z, core), tp: 16 (over y, x).
Axes of the slice: x: 4, y: 4, z: 16, core: 2. Of those that a mesh axis runs over, the one named last changes fastest.
Arguments:
- mixer_value_input: bfloat16 [8192, 4096], P('ep', 'tp'), may hold values from -6 to 6
- input_state_matrix: bfloat16 [8192, 2048], P('ep', 'tp'), may hold values from -6 to 6
- output_state_matrix: bfloat16 [8192, 2048], P('ep', 'tp'), may hold values from -6 to 6
- output_gate_input: bfloat16 [8192, 4096], P('ep', 'tp'), may hold values from -6 to 6
- step_input: float32 [8192, 64], P('ep', 'tp'), may hold values from -6 to -2
- extra_log_decay: float32 [8192, 64], P('ep', 'tp'), may hold values from -1 to 0
- head_log_decay: float32 [64], P('tp'), may hold values from -10 to 1
- head_skip_scale: float32 [64], P('tp'), may hold values from 0.5 to 2
- value_kernel: float32 [4, 4096], P(None, 'tp'), may hold values from -3 to 3
- input_matrix_kernel: float32 [4, 2048], P(None, 'tp'), may hold values from -3 to 3
- output_matrix_kernel: float32 [4, 2048], P(None, 'tp'), may hold values from -3 to 3
- mixer_norm_scale: float32 [4096], P('tp'), may hold values from 0.1 to 1.9
- mixer_output_weight: bfloat16 [4096, 2048], P(None, 'tp'), may hold values from -0.09375 to 0.09375
- second_token_rows: bfloat16 [8192, 2048], P('ep'), may hold values from -6 to 6
- expert_norm_scale: float32 [2048], replicated, may hold values from 0.1 to 1.9
- routed_expert_index: int32 [8192, 4], P('ep'), may hold values from 0 to 63, all different within a row; in each aligned block of 256 rows (0 to 255, 256 to 511, ...) at most 24 rows name the same one
- routed_expert_weight: float32 [8192, 4], P('ep'), may hold values from 0.1 to 1
- routed_gate_weight: bfloat16 [64, 2048, 1024], P('ep', None, 'tp'), may hold values from -0.125 to 0.125
- routed_up_weight: bfloat16 [64, 2048, 1024], P('ep', None, 'tp'), may hold values from -0.125 to 0.125
- routed_down_weight: bfloat16 [64, 1024, 2048], P('ep', None, 'tp'), may hold values from -0.1875 to 0.1875
- shared_gate_weight: bfloat16 [2048, 1024], P(None, 'tp'), may hold values from -0.125 to 0.125
- shared_up_weight: bfloat16 [2048, 1024], P(None, 'tp'), may hold values from -0.125 to 0.125
- shared_down_weight: bfloat16 [1024, 2048], P(None, 'tp'), may hold values from -0.1875 to 0.1875
Outputs:
- mixer_output: bfloat16 [8192, 2048], P('ep', 'tp')
- routed_out: bfloat16 [8192, 2048], P('ep', 'tp')
Inputs may be any that keep to these rules, and one draw needn't show every extreme that they name: `routed_expert_index`: in each aligned block of 256 rows (the rows of one index of ep) no expert is named more than 24 times, a bound that some block reaches.
All inputs are finite; a program needn't handle non-finite values.
Results may differ from a plain program's by a relative error of at most 0.012.
Values may be sent and summed in bfloat16 or wider, within the bound.
No kernel may reach another device: no remote copies, remote signals or barrier semaphores. Data moves between devices by JAX's collectives and lax.ppermute only.
A program may use at most 64 MiB of HBM per device.

v0:
```python
import jax
import jax.numpy as jnp
from jax import lax
from jax.sharding import PartitionSpec as P

HEAD_DIM = 64
STATE = 128
CONV_TAPS = 4
BLOCK = 128
TOP_K = 4
epsilon = 1e-05
F32 = jnp.float32
BF16 = jnp.bfloat16


def passed_along(x, axis, by):
    size = lax.axis_size(axis)
    pairs = [(i, i + by) for i in range(size) if 0 <= i + by < size]
    return lax.ppermute(x, axis, pairs)


def high(x):
    return lax.reduce_precision(x, 8, 7)


def three_parts(x):
    a = high(x)
    b = high(x - a)
    return (a, b, x - a - b)


def laid_out(tiles, dim):
    tiles = jnp.moveaxis(tiles, 0, dim)
    dims = tiles.shape
    return tiles.reshape(*dims[:dim], dims[dim] * dims[dim + 1], *dims[dim + 2 :])


def one_gather(arrays, axis, dims):
    ravelled = jnp.concatenate([a.reshape(-1) for a in arrays])
    lines, at, finished = (lax.all_gather(ravelled, axis), 0, [])
    for a, dim in zip(arrays, dims):
        tiles = lines[:, at : at + a.size].reshape(-1, *a.shape)
        finished.append(laid_out(tiles, dim))
        at += a.size
    return tuple(finished)


def conv_silu(tail_rows, source, weights):
    length = source.shape[0]
    padded = jnp.concatenate([tail_rows, source], axis=0)
    total_sum = jnp.zeros(source.shape, F32)
    for tap_index in range(CONV_TAPS):
        total_sum = (
            total_sum + padded[tap_index : tap_index + length].astype(F32) * weights[tap_index]
        )
    return jax.nn.silu(total_sum).astype(BF16)


def state_before(log_total, total_state):
    heads = log_total.shape[0]
    count = lax.axis_size("ep")
    place = lax.axis_index("ep")
    parts = jnp.stack(three_parts(log_total)).reshape(1, 3 * heads)
    row = jnp.pad(parts, ((0, 15), (0, STATE - 3 * heads)))
    rows = heads * HEAD_DIM
    payload = jnp.concatenate([total_state.reshape(rows, STATE), row], axis=0).astype(BF16)
    gathered = lax.all_gather(payload, "ep")
    tail = gathered[:, rows, : 3 * heads].astype(F32).reshape(count, 3, heads)
    logs = jnp.sum(tail, axis=1)
    at = jnp.arange(count)
    between = (at[None, :] > at[:, None]) & (at[None, :] < place)
    spans = jnp.sum(jnp.where(between[:, :, None], logs[None], 0.0), axis=1)
    weights = jnp.where((at < place)[:, None], jnp.exp(spans), 0.0)
    wide = jnp.repeat(weights, HEAD_DIM, axis=1)[:, :, None]
    summed = jnp.sum(gathered[:, :rows, :].astype(F32) * wide, axis=0)
    return summed.reshape(heads, HEAD_DIM, STATE)


def routes(index_t, weight_t, experts, capacity):
    rows = index_t.shape[1]
    ids = jnp.arange(experts, dtype=jnp.int32)[:, None]
    named = jnp.zeros((experts, rows), F32)
    weight = jnp.zeros((experts, rows), F32)
    for k in range(TOP_K):
        hit = index_t[k][None, :] == ids
        named = jnp.where(hit, 1.0, named)
        weight = jnp.where(hit, weight_t[k][None, :], weight)
    at = jnp.arange(rows)
    earlier = (at[:, None] < at[None, :]).astype(BF16)
    place = jnp.dot(named.astype(BF16), earlier, preferred_element_type=F32)
    place = jnp.where(named > 0.0, place, -1.0)
    slots = jnp.arange(capacity, dtype=jnp.int32).astype(F32)[None, :, None]
    taken = place[:, None, :] == slots
    return (taken, weight)


def on_device(
    mixer_value_input,
    input_state_matrix,
    output_state_matrix,
    output_gate_input,
    step_input,
    extra_log_decay,
    head_log_decay,
    head_skip_scale,
    value_kernel,
    input_matrix_kernel,
    output_matrix_kernel,
    mixer_norm_scale,
    mixer_output_weight,
    second_token_rows,
    expert_norm_scale,
    routed_expert_index,
    routed_expert_weight,
    routed_gate_weight,
    routed_up_weight,
    routed_down_weight,
    shared_gate_weight,
    shared_up_weight,
    shared_down_weight,
):
    length = mixer_value_input.shape[0]
    heads_local = step_input.shape[1]
    width_x = mixer_value_input.shape[1]
    width_b = input_state_matrix.shape[1]
    groups_local = width_b // STATE
    head_ratio = heads_local // groups_local
    nblocks = length // BLOCK
    lead_row = length - CONV_TAPS + 1
    edge_rows = jnp.concatenate(
        [
            mixer_value_input[lead_row:],
            input_state_matrix[lead_row:],
            output_state_matrix[lead_row:],
        ],
        axis=1,
    )
    tail_rows = passed_along(edge_rows, "ep", 1)
    values = conv_silu(tail_rows[:, :width_x], mixer_value_input, value_kernel)
    in_mat = conv_silu(
        tail_rows[:, width_x : width_x + width_b], input_state_matrix, input_matrix_kernel
    )
    out_mat = conv_silu(
        tail_rows[:, width_x + width_b :], output_state_matrix, output_matrix_kernel
    )
    step_length = jax.nn.softplus(step_input)
    decay_logarithm = -jnp.exp(head_log_decay)[None, :] * step_length + extra_log_decay
    running = jnp.cumsum(decay_logarithm.reshape(nblocks, BLOCK, heads_local), axis=1)
    value_wide = values.astype(F32).reshape(nblocks, BLOCK, heads_local, HEAD_DIM)
    scaled = value_wide * step_length.reshape(nblocks, BLOCK, heads_local)[..., None]
    in_blocks = in_mat.reshape(nblocks, BLOCK, groups_local, STATE)
    out_blocks = out_mat.reshape(nblocks, BLOCK, groups_local, STATE)
    scores = jnp.einsum("bign,bjgn->bgij", out_blocks, in_blocks, preferred_element_type=F32)
    scores = jnp.repeat(scores, head_ratio, axis=1)
    spread = jnp.transpose(running[:, :, None, :] - running[:, None, :, :], (0, 3, 1, 2))
    lower_mask = jnp.tril(jnp.ones((BLOCK, BLOCK), bool))[None, None]
    decay_mat = jnp.where(lower_mask, jnp.exp(jnp.where(lower_mask, spread, 0.0)), 0.0)
    inside = jnp.einsum("bhij,bjhp->bihp", scores * decay_mat, scaled)
    out_head = jnp.repeat(out_blocks.astype(F32), head_ratio, axis=2)
    in_head = jnp.repeat(in_blocks.astype(F32), head_ratio, axis=2)
    block_logs = running[:, -1]
    to_end = jnp.exp(block_logs[:, None, :] - running)
    block_state = jnp.einsum("bjhn,bjh,bjhp->bhpn", in_head, to_end, scaled)
    carried = jnp.zeros((heads_local, HEAD_DIM, STATE), F32)
    before = []
    for b in range(nblocks):
        before.append(carried)
        carried = carried * jnp.exp(block_logs[b])[:, None, None] + block_state[b]
    local_prev = jnp.stack(before)
    before_logs = jnp.cumsum(block_logs, axis=0) - block_logs
    incoming = state_before(jnp.sum(block_logs, axis=0), carried)
    entering = local_prev + jnp.exp(before_logs)[:, :, None, None] * incoming[None]
    carried_term = jnp.einsum("bihn,bhpn->bihp", out_head, entering) * jnp.exp(running)[..., None]
    mixed_heads = (inside + carried_term).reshape(length, heads_local, HEAD_DIM)
    mixed_heads = mixed_heads + head_skip_scale[None, :, None] * value_wide.reshape(
        length, heads_local, HEAD_DIM
    )
    gated_heads = mixed_heads * jax.nn.silu(output_gate_input.astype(F32)).reshape(
        length, heads_local, HEAD_DIM
    )
    grouped = gated_heads.reshape(length, groups_local, head_ratio * HEAD_DIM)
    grouped = grouped * lax.rsqrt(jnp.mean(grouped * grouped, axis=-1, keepdims=True) + epsilon)
    mixer_normed = (grouped.reshape(length, width_x) * mixer_norm_scale).astype(BF16)
    rows_local = second_token_rows.shape[0]
    model_width = second_token_rows.shape[1]
    local_experts = routed_gate_weight.shape[0]
    ep_count = lax.axis_size("ep")
    experts = local_experts * ep_count
    capacity = max(2, 3 * rows_local * TOP_K // (2 * experts))
    col_width = model_width // lax.axis_size("tp")
    rows_wide = second_token_rows.astype(F32)
    normed = (
        rows_wide
        * lax.rsqrt(jnp.mean(rows_wide * rows_wide, axis=-1, keepdims=True) + epsilon)
        * expert_norm_scale
    ).astype(BF16)
    taken, weight = routes(routed_expert_index.T, routed_expert_weight.T, experts, capacity)
    one_hot = taken.astype(BF16).reshape(experts * capacity, rows_local)
    mine = lax.dynamic_slice_in_dim(normed, lax.axis_index("tp") * col_width, col_width, 1)
    my_columns = jnp.dot(one_hot, mine, preferred_element_type=F32).astype(BF16)
    my_columns = my_columns.reshape(experts, capacity, col_width)
    arrived = lax.all_to_all(my_columns, "ep", split_axis=0, concat_axis=1, tiled=True)
    column_piece = lax.all_gather(arrived, "tp", axis=2, tiled=True)
    gate_pre = jnp.einsum(
        "esd,edf->esf", column_piece, routed_gate_weight, preferred_element_type=F32
    )
    up_pre = jnp.einsum("esd,edf->esf", column_piece, routed_up_weight, preferred_element_type=F32)
    hidden = (jax.nn.silu(gate_pre) * up_pre).astype(BF16)
    shared_hidden = (
        jax.nn.silu(jnp.dot(normed, shared_gate_weight, preferred_element_type=F32))
        * jnp.dot(normed, shared_up_weight, preferred_element_type=F32)
    ).astype(BF16)
    whole_mix, whole_hidden, whole_shared = one_gather(
        (mixer_normed, hidden, shared_hidden), "tp", (1, 2, 1)
    )
    mixer_output = jnp.dot(whole_mix, mixer_output_weight, preferred_element_type=F32).astype(BF16)
    expert_result = jnp.einsum(
        "esf,efd->esd", whole_hidden, routed_down_weight, preferred_element_type=F32
    ).astype(BF16)
    returned = lax.all_to_all(expert_result, "ep", split_axis=1, concat_axis=0, tiled=True)
    returned = returned.reshape(experts * capacity, col_width)
    weight_high = high(weight)
    contract = (((0,), (0,)), ((), ()))
    routed_sum = jnp.zeros((rows_local, col_width), F32)
    for part in (weight_high, weight - weight_high):
        spread_part = jnp.where(taken, part[:, None, :], 0.0).astype(BF16)
        spread_part = spread_part.reshape(experts * capacity, rows_local)
        routed_sum = routed_sum + lax.dot_general(
            spread_part, returned, contract, preferred_element_type=F32
        )
    shared_result = jnp.dot(whole_shared, shared_down_weight, preferred_element_type=F32)
    routed_out = (routed_sum + shared_result).astype(BF16)
    return (mixer_output, routed_out)


def solution(mesh):
    return jax.shard_map(
        on_device,
        mesh=mesh,
        in_specs=(
            P("ep", "tp"),
            P("ep", "tp"),
            P("ep", "tp"),
            P("ep", "tp"),
            P("ep", "tp"),
            P("ep", "tp"),
            P("tp"),
            P("tp"),
            P(None, "tp"),
            P(None, "tp"),
            P(None, "tp"),
            P("tp"),
            P(None, "tp"),
            P("ep", None),
            P(),
            P("ep", None),
            P("ep", None),
            P("ep", None, "tp"),
            P("ep", None, "tp"),
            P("ep", None, "tp"),
            P(None, "tp"),
            P(None, "tp"),
            P(None, "tp"),
        ),
        out_specs=(P("ep", "tp"), P("ep", "tp")),
        check_vma=False,
    )
```

profile of v0, /device:TPU:1, one launch (start us, length us, event | category | flops | bytes accessed | tf_op | source)
XLA Modules:
  0.0 346.0 jit_solution(6306174903025940382)
XLA Ops:
  7.2 0.8 slice.140
  8.0 0.7 slice.141
  8.7 0.7 slice.139
  9.6 4.9 %collective-permute-start = (bf16[3,512]{0,1:T(8,128)(2,1)S(1)}, bf16[3,512]{0,1:T(8,128)(2,1)S(1)}, u32[]{:S(2)}, u32[]{:S(2)}) collective-permute-start(bf16[3,512]{0,1:T(8,128)(2,1)S(1)} %copy.162), channel_id=1, source_target_pairs={{0,16},{16,32},{32,48},{48,64},{64,80},{80,96},{96,112},{112,128},... | collective-permute-start | bytes 9224 | tf_op jit(solution)/shard_map/ppermute | solution.py:19
  14.5 0.7 exponential_negate_fusion
  15.2 0.8 compare_select_fusion.2
  16.3 0.8 slice_bitcast_fusion.3
  17.2 0.8 fusion.70
  18.1 0.7 fusion.67
  18.8 1.0 copy.163
  20.2 0.6 fusion.68
  21.0 0.4 fusion.38
  21.5 0.8 broadcast_multiply_fusion
  22.6 0.8 fusion.66
  23.5 0.6 pad_maximum_fusion.2
  25.6 0.4 convolution_convert_fusion
  26.0 44.8 %all_to_all.33 = bf16[64,24,128]{2,1,0:T(8,128)(2,1)S(1)} all-to-all(bf16[64,24,128]{2,1,0:T(8,128)(2,1)S(1)} %bitcast.139), channel_id=1, replica_groups=mesh['ep'=32,'tp'=16] {'ep'}, dimensions={0} | all-to-all | bytes 786432 | tf_op jit(solution)/shard_map/all_to_all | solution.py:202
  70.8 0.8 copy.179
  72.1 1.4 fusion.74
  73.6 1.4 fusion.9
  75.7 28.7 %all-gather.5.cloned.1.call-done = bf16[32,272,128]{2,1,0:T(8,128)(2,1)} async-done(((bf16[1,272,128]{2,1,0:T(8,128)(2,1)}), bf16[32,272,128]{2,1,0:T(8,128)(2,1)}) %all-gather.5.cloned.1.call-update) | async-done | bytes 2228240 | tf_op jit(solution)/shard_map/all_gather | solution.py:67
  104.4 0.8 slice.205
  105.8 3.3 multiply_reduce_fusion
  109.1 0.3 fusion.6
  109.5 0.4 fusion.7
  110.6 73.3 %all-gather.7.cloned.1.call-done = bf16[2,768,2048]{2,1,0:T(8,128)(2,1)} async-done(((bf16[2,768,128]{2,1,0:T(8,128)(2,1)}), bf16[2,768,2048]{2,1,0:T(8,128)(2,1)}) %all-gather.7.cloned.1.call-update) | async-done | bytes 6291472 | tf_op jit(solution)/shard_map/all_gather | solution.py:203
  183.9 5.0 %fusion.73 = f32[2,768,64]{1,2,0:T(8,128)S(1)} fusion(bf16[2,768,2048]{2,1,0:T(8,128)(2,1)} %all-gather.7.cloned.1.call-done, bf16[2,2048,64]{1,2,0:T(8,128)(2,1)S(1)} %copy-done.8), kind=kOutput, calls=%fused_computation.151 | convolution fusion | flops 402653184 | bytes 7208960 | tf_op jit(solution)/shard_map/esd,edf->esf/dot_general | solution.py:204
  188.9 2.0 fusion.5
  191.3 0.8 pad_maximum_fusion
  192.1 74.8 %all-gather.9.cloned.1.call-done = bf16[2883584]{0:T(1024)(128)(2,1)} async-done(((bf16[180224]{0:T(1024)(128)(2,1)}), bf16[2883584]{0:T(1024)(128)(2,1)}) %all-gather.9.cloned.1.call-update) | async-done | bytes 5767184 | tf_op jit(solution)/shard_map/all_gather | solution.py:40
  266.9 5.8 %reshape.648 = bf16[16,180224]{1,0:T(8,128)(2,1)} reshape(bf16[2883584]{0:T(1024)(128)(2,1)} %all-gather.9.cloned.1.call-done) | data formatting | bytes 11534336 | tf_op jit(solution)/shard_map/all_gather | solution.py:40
  272.7 3.7 %slice.215 = bf16[16,98304]{1,0:T(8,128)(2,1)} slice(bf16[16,180224]{1,0:T(8,128)(2,1)} %reshape.648), slice={[0:16], [65536:163840]} | slice | bytes 6291456 | tf_op jit(solution)/shard_map/slice | solution.py:42
  276.4 8.8 %reshape.642 = bf16[16,2,768,64]{3,2,1,0:T(8,128)(2,1)} reshape(bf16[16,98304]{1,0:T(8,128)(2,1)} %slice.215) | data formatting | bytes 6291456 | tf_op jit(solution)/shard_map/reshape | solution.py:42
  285.3 6.9 %copy.183 = bf16[2,768,16,64]{1,3,2,0:T(8,128)(2,1)} copy(bf16[2,768,16,64]{3,1,0,2:T(8,128)(2,1)} %bitcast.127) | data formatting | bytes 6291456 | tf_op jit(solution)/shard_map/transpose | solution.py:33
  292.2 3.3 convolution_convert_fusion.1
  295.5 1.2 copy.185
  296.6 13.2 %all-to-all-start.1 = ((bf16[2,768,128]{2,0,1:T(2,128)(2,1)}), bf16[2,768,128]{2,0,1:T(2,128)(2,1)S(1)}, u32[]{:S(2)}, u32[]{:S(2)}) async-start(bf16[2,768,128]{2,0,1:T(2,128)(2,1)} %copy.185), calls=%async_computation.1 | async-start | bytes 786432 | tf_op jit(solution)/shard_map/all_to_all | solution.py:220
  309.9 1.8 fusion.4
  311.7 3.1 slice.210
  314.8 1.1 reshape.645
  316.0 1.1 copy.188
  317.1 2.0 copy.194
  319.2 2.4 copy.182
  321.6 3.0 convolution_convert_fusion.2
  324.6 12.9 %all-to-all-done.1 = bf16[2,768,128]{2,0,1:T(2,128)(2,1)S(1)} async-done(((bf16[2,768,128]{2,0,1:T(2,128)(2,1)}), bf16[2,768,128]{2,0,1:T(2,128)(2,1)S(1)}, u32[]{:S(2)}, u32[]{:S(2)}) %all-to-all-start.1) | async-done | bytes 393248 | tf_op jit(solution)/shard_map/all_to_all | solution.py:220
  337.7 0.4 fusion.75
  338.1 0.4 convolution_add_fusion.1
  338.5 1.0 fusion.8
  (146 shorter events, 6.0 us)
Async XLA Ops:
  7.2 314.4 %copy-start = (bf16[4096,128]{1,0:T(8,128)(2,1)S(1)}, bf16[4096,128]{1,0:T(8,128)(2,1)}, u32[]{:S(2)}) copy-start(bf16[4096,128]{1,0:T(8,128)(2,1)} %param.35) | copy-start | bytes 3145732
  7.2 15.1 %copy-start.18 = (bf16[256,128]{1,0:T(8,128)(2,1)S(1)}, bf16[256,128]{1,0:T(8,128)(2,1)}, u32[]{:S(2)}) copy-start(bf16[256,128]{1,0:T(8,128)(2,1)} %param.24) | copy-start | bytes 196612
  7.2 97.2 %all-gather.5.cloned.1.call-start = ((), (), s32[]{:S(2)}) async-start(), calls=%async_computation.2 | async-start | bytes 2297856 | tf_op jit(solution)/shard_map/all_gather | solution.py:67
  9.6 10.7 %collective-permute-start = (bf16[3,512]{0,1:T(8,128)(2,1)S(1)}, bf16[3,512]{0,1:T(8,128)(2,1)S(1)}, u32[]{:S(2)}, u32[]{:S(2)}) collective-permute-start(bf16[3,512]{0,1:T(8,128)(2,1)S(1)} %copy.162), channel_id=1, source_target_pairs={{0,16},{16,32},{32,48},{48,64},{64,80},{80,96},{96,112},{112,128},... | collective-permute-start | bytes 9224 | tf_op jit(solution)/shard_map/ppermute | solution.py:19
  18.1 6.2 %copy-start.27 = (s32[256,4]{0,1:T(4,128)S(1)}, s32[256,4]{0,1:T(4,128)}, u32[]{:S(2)}) copy-start(s32[256,4]{0,1:T(4,128)} %param.38) | copy-start | bytes 12292
  20.9 3.9 %copy-start.2 = (bf16[256,2048]{1,0:T(8,128)(2,1)S(1)}, bf16[256,2048]{1,0:T(8,128)(2,1)}, u32[]{:S(2)}) copy-start(bf16[256,2048]{1,0:T(8,128)(2,1)} %param.36) | copy-start | bytes 3145732
  21.5 3.7 %copy-start.20 = (f32[2048]{0:T(1024)S(1)}, f32[2048]{0:T(1024)}, u32[]{:S(2)}) copy-start(f32[2048]{0:T(1024)} %param.37) | copy-start | bytes 24580
  22.4 1.0 copy-start.6
  24.2 159.7 %all-gather.7.cloned.1.call-start = ((), (), s32[]{:S(2)}) async-start(), calls=%async_computation.3 | async-start | bytes 6684672 | tf_op jit(solution)/shard_map/all_gather | solution.py:203
  24.2 0.9 copy-start.29
  24.4 0.8 copy-start.21
  24.4 0.8 copy-start.23
  24.4 0.8 copy-start.25
  24.6 0.6 copy-start.12
  25.5 46.2 %copy-start.33 = (f32[4]{0:T(128)S(1)}, f32[4]{0:T(128)}, u32[]{:S(2)}) copy-start(f32[4]{0:T(128)} %param.30) | copy-start | bytes 52
  25.6 46.4 %copy-start.15 = (bf16[256,256]{1,0:T(8,128)(2,1)S(1)}, bf16[256,256]{1,0:T(8,128)(2,1)}, u32[]{:S(2)}) copy-start(bf16[256,256]{1,0:T(8,128)(2,1)} %param.26) | copy-start | bytes 393220
  25.6 46.5 %copy-start.9 = (f32[2,128,4]{2,1,0:T(8,128)S(1)}, f32[2,128,4]{2,1,0:T(8,128)}, u32[]{:S(2)}) copy-start(f32[2,128,4]{2,1,0:T(8,128)} %get-tuple-element.13) | copy-start | bytes 12292
  70.8 4.5 %copy-start.31 = (f32[4,128]{1,0:T(4,128)S(1)}, f32[4,128]{1,0:T(4,128)}, u32[]{:S(2)}) copy-start(f32[4,128]{1,0:T(4,128)} %param.33) | copy-start | bytes 6148
  70.8 4.5 %copy-start.16 = (bf16[3,128]{0,1:T(8,128)(2,1)S(1)}, bf16[3,128]{0,1:T(8,128)(2,1)}, u32[]{:S(2)}) copy-start(bf16[3,128]{0,1:T(8,128)(2,1)} %get-tuple-element.16) | copy-start | bytes 2308
  70.8 4.6 %copy-start.19 = (bf16[256,128]{1,0:T(8,128)(2,1)S(1)}, bf16[256,128]{1,0:T(8,128)(2,1)}, u32[]{:S(2)}) copy-start(bf16[256,128]{1,0:T(8,128)(2,1)} %param.25) | copy-start | bytes 196612
  71.6 3.9 %copy-start.7 = (bf16[256,128]{1,0:T(8,128)(2,1)S(1)}, bf16[256,128]{1,0:T(8,128)(2,1)}, u32[]{:S(2)}) copy-start(bf16[256,128]{1,0:T(8,128)(2,1)} %copy-done.6) | copy-start | bytes 196612
  71.6 195.3 %all-gather.9.cloned.1.call-start = ((), (), s32[]{:S(2)}) async-start(), calls=%async_computation.4 | async-start | bytes 6127616 | tf_op jit(solution)/shard_map/all_gather | solution.py:40
  73.5 35.6 %copy-start.10 = (f32[1,4,64,128]{3,2,1,0:T(8,128)S(1)}, f32[1,4,64,128]{3,2,1,0:T(8,128)}, u32[]{:S(2)}) copy-start(f32[1,4,64,128]{3,2,1,0:T(8,128)} %get-tuple-element.7) | copy-start | bytes 393220
  75.0 34.5 %copy-start.17 = (bf16[2,128,4,64]{1,0,3,2:T(2,128)(2,1)S(1)}, bf16[2,128,4,64]{1,0,3,2:T(2,128)(2,1)}, u32[]{:S(2)}) copy-start(bf16[2,128,4,64]{1,0,3,2:T(2,128)(2,1)} %get-tuple-element.5) | copy-start | bytes 393220
  105.8 4.5 %copy-start.32 = (f32[256]{0:T(256)S(1)}, f32[256]{0:T(256)}, u32[]{:S(2)}) copy-start(f32[256]{0:T(256)} %param.34) | copy-start | bytes 3076
  109.1 74.8 %copy-start.8 = (bf16[2,2048,64]{1,2,0:T(8,128)(2,1)S(1)}, bf16[2,2048,64]{1,2,0:T(8,128)(2,1)}, u32[]{:S(2)}) copy-start(bf16[2,2048,64]{1,2,0:T(8,128)(2,1)} %param.40) | copy-start | bytes 1572868
  110.6 78.3 %copy-start.34 = (bf16[2,2048,64]{1,2,0:T(8,128)(2,1)S(1)}, bf16[2,2048,64]{1,2,0:T(8,128)(2,1)}, u32[]{:S(2)}) copy-start(bf16[2,2048,64]{1,2,0:T(8,128)(2,1)} %param.41) | copy-start | bytes 1572868
  183.9 5.0 %copy-start.1 = (bf16[2,768,2048]{2,1,0:T(8,128)(2,1)S(1)}, bf16[2,768,2048]{2,1,0:T(8,128)(2,1)}, u32[]{:S(2)}) copy-start(bf16[2,768,2048]{2,1,0:T(8,128)(2,1)} %all-gather.7.cloned.1.call-done) | copy-start | bytes 18874372
  285.3 6.9 %copy-start.11 = (bf16[2,1024,128]{2,1,0:T(8,128)(2,1)S(1)}, bf16[2,1024,128]{2,1,0:T(8,128)(2,1)}, u32[]{:S(2)}) copy-start(bf16[2,1024,128]{2,1,0:T(8,128)(2,1)} %param.42) | copy-start | bytes 1572868
  292.2 17.7 %copy-start.28 = (f32[256,4]{0,1:T(4,128)S(1)}, f32[256,4]{0,1:T(4,128)}, u32[]{:S(2)}) copy-start(f32[256,4]{0,1:T(4,128)} %param.39) | copy-start | bytes 12292
  292.2 17.7 %copy-start.22 = (s32[1,256]{1,0:T(1,128)S(1)}, s32[1,256]{1,0:T(1,128)}, u32[]{:S(2)}) copy-start(s32[1,256]{1,0:T(1,128)} %copy-done.21) | copy-start | bytes 3076
  292.2 17.7 %copy-start.24 = (s32[1,256]{1,0:T(1,128)S(1)}, s32[1,256]{1,0:T(1,128)}, u32[]{:S(2)}) copy-start(s32[1,256]{1,0:T(1,128)} %copy-done.23) | copy-start | bytes 3076
  292.2 17.7 %copy-start.26 = (s32[1,256]{1,0:T(1,128)S(1)}, s32[1,256]{1,0:T(1,128)}, u32[]{:S(2)}) copy-start(s32[1,256]{1,0:T(1,128)} %copy-done.25) | copy-start | bytes 3076
  292.2 17.7 %copy-start.13 = (f32[64,256]{1,0:T(8,128)S(1)}, f32[64,256]{1,0:T(8,128)}, u32[]{:S(2)}) copy-start(f32[64,256]{1,0:T(8,128)} %copy-done.12) | copy-start | bytes 196612
  292.2 17.7 %copy-start.30 = (f32[24]{0:T(128)S(1)}, f32[24]{0:T(128)}, u32[]{:S(2)}) copy-start(f32[24]{0:T(128)} %copy-done.29) | copy-start | bytes 292
  296.6 40.9 %all-to-all-start.1 = ((bf16[2,768,128]{2,0,1:T(2,128)(2,1)}), bf16[2,768,128]{2,0,1:T(2,128)(2,1)S(1)}, u32[]{:S(2)}, u32[]{:S(2)}) async-start(bf16[2,768,128]{2,0,1:T(2,128)(2,1)} %copy.185), calls=%async_computation.1 | async-start | bytes 786432 | tf_op jit(solution)/shard_map/all_to_all | solution.py:220
  311.7 3.1 slice-start
  321.6 16.1 %copy-start.3 = (bf16[64,24,256]{2,1,0:T(8,128)(2,1)S(1)}, bf16[64,24,256]{2,1,0:T(8,128)(2,1)}, u32[]{:S(2)}) copy-start(bf16[64,24,256]{2,1,0:T(8,128)(2,1)} %get-tuple-element.18) | copy-start | bytes 2359300
  324.6 13.4 %copy-start.4 = (bf16[64,24,256]{2,1,0:T(8,128)(2,1)S(1)}, bf16[64,24,256]{2,1,0:T(8,128)(2,1)}, u32[]{:S(2)}) copy-start(bf16[64,24,256]{2,1,0:T(8,128)(2,1)} %get-tuple-element.17) | copy-start | bytes 2359300
  324.6 13.9 %copy-start.5 = (bf16[256,16,64]{0,2,1:T(8,128)(2,1)S(1)}, bf16[256,16,64]{0,2,1:T(8,128)(2,1)}, u32[]{:S(2)}) copy-start(bf16[256,16,64]{0,2,1:T(8,128)(2,1)} %copy.188) | copy-start | bytes 1572868
  337.5 1.0 copy-start.14
Sparse Core Ops, SparseCore 0:
  24.3 80.0 all-gather.4
  107.4 76.4 all-gather.6
  192.2 74.6 all-gather.8
where the time goes:
time: 347 us; the launch traced here: 346 us
  waiting for transfers between devices  190 us (55%)
  local copies, waits for them, and re-layouts  46.7 us (13%)
  blocking collectives  44.8 us (13%)
  matrix products  19.5 us (6%)
  starting transfers between devices  18.2 us (5%)
  between operations  14.5 us (4%)
  other arithmetic  12.5 us (4%)
    all_gather x1, waiting for transfers between devices, one_gather(): lines, at, finished = (lax.all_gather(ravelled, axis), 0, [])  74.8 us
    all_gather x1, waiting for transfers between devices, on_device(): column_piece = lax.all_gather(arrived, 'tp', axis=2, tiled=True)  73.3 us
    all_to_all x1, blocking collectives, on_device(): lax.all_to_all(my_columns, 'ep', split_axis=0, concat_axis=1, tiled=True)  44.8 us
    all_gather x1, waiting for transfers between devices, state_before(): gathered = lax.all_gather(payload, 'ep')  28.7 us
    all_to_all x1, starting transfers between devices, on_device(): lax.all_to_all(expert_result, 'ep', split_axis=1, concat_axis=0, tiled=True)  13.2 us
    all_to_all x1, waiting for transfers between devices, on_device(): lax.all_to_all(expert_result, 'ep', split_axis=1, concat_axis=0, tiled=True)  12.9 us
    transpose x3, local copies, waits for them, and re-layouts, laid_out(): tiles = jnp.moveaxis(tiles, 0, dim)  10.4 us
    reshape x2, local copies, waits for them, and re-layouts, one_gather(): tiles = lines[:, at:at + a.size].reshape(-1, *a.shape)  9.96 us
  transfers between devices with their start and end apart: 5, of which 4 were waited for; matrix products, arithmetic and copies ran while one was open for 9% of the time, Pallas kernels for 0%

commit v1 on v0

--- a/solution.py
+++ b/solution.py
@@ -200,7 +200,19 @@
     my_columns = jnp.dot(one_hot, mine, preferred_element_type=F32).astype(BF16)
     my_columns = my_columns.reshape(experts, capacity, col_width)
     arrived = lax.all_to_all(my_columns, "ep", split_axis=0, concat_axis=1, tiled=True)
-    column_piece = lax.all_gather(arrived, "tp", axis=2, tiled=True)
+    dev_count = lax.axis_size("tp")
+    buffers = tuple(((m, (m + 1) % dev_count) for m in range(dev_count)))
+    in_order = tuple(((m, (m - 1) % dev_count) for m in range(dev_count)))
+    res, t_next = ([arrived], [arrived])
+    for _ in range(dev_count // 2):
+        res.append(lax.ppermute(res[-1], axis_name="tp", perm=buffers))
+    for _ in range((dev_count - 1) // 2):
+        t_next.append(lax.ppermute(t_next[-1], axis_name="tp", perm=in_order))
+    column_piece = jnp.roll(
+        jnp.concatenate([*res[::-1], *t_next[1:]], axis=2),
+        (lax.axis_index("tp") - dev_count // 2) * arrived.shape[2],
+        axis=2,
+    )
     gate_pre = jnp.einsum(
         "esd,edf->esf", column_piece, routed_gate_weight, preferred_element_type=F32
     )

time: 347 us -> 362 us (1.043)
  starting transfers between devices: 18.2 us -> 97.3 us
  waiting for transfers between devices: 190 us -> 119 us
  blocking collectives: 44.8 us -> 0 us
  local copies, waits for them, and re-layouts: 46.7 us -> 84 us
  other arithmetic: 12.5 us -> 21.2 us
    all_gather x1 -> x0, waiting for transfers between devices: 73.3 us -> none  [on_device(): column_piece = lax.all_gather(arrived, 'tp', axis=2, tiled=True)]
    ppermute x0 -> x15, starting transfers between devices: none -> 63.8 us  [the longest x7 47.1 us: on_device(): t_next.append(lax.ppermute(t_next[-1], axis_name='tp', perm=in_order))]
    all_to_all x1 -> x0, blocking collectives: 44.8 us -> none  [on_device(): lax.all_to_all(my_columns, 'ep', split_axis=0, concat_axis=1, tiled=True)]
    all_gather x1, waiting for transfers between devices: 28.7 us -> 0.02 us  [state_before(): gathered = lax.all_gather(payload, 'ep')]
    unnamed x75 -> x60, local copies, waits for them, and re-layouts: 3.53 us -> 30.4 us
    ppermute x0 -> x15, waiting for transfers between devices: none -> 20.9 us  [the longest x8 18 us: on_device(): res.append(lax.ppermute(res[-1], axis_name='tp', perm=buffers))]
    all_to_all x0 -> x1, starting transfers between devices: none -> 16.7 us  [on_device(): lax.all_to_all(my_columns, 'ep', split_axis=0, concat_axis=1, tiled=True)]
    ppermute x1, waiting for transfers between devices: 0.01 us -> 5.74 us  [passed_along(): return lax.ppermute(x, axis, pairs)]
  transfers between devices with their start and end apart: 5 -> 20, of which waited for: 4 -> 12; matrix products, arithmetic and copies ran while one was open for 9% -> 19% of each run, Pallas kernels for 0% -> 0%
where the time goes in v1:
time: 362 us; the launch traced here: 359 us
  waiting for transfers between devices  119 us (33%)
  starting transfers between devices  97.3 us (27%)
  local copies, waits for them, and re-layouts  84 us (23%)
  matrix products  23.1 us (6%)
  other arithmetic  21.2 us (6%)
  between operations  14.9 us (4%)
    all_gather x1, waiting for transfers between devices, one_gather(): lines, at, finished = (lax.all_gather(ravelled, axis), 0, [])  75.9 us
    ppermute x7, starting transfers between devices, on_device(): t_next.append(lax.ppermute(t_next[-1], axis_name='tp', perm=in_order))  47.1 us
    unnamed x60, local copies, waits for them, and re-layouts  30.4 us
    ppermute x8, waiting for transfers between devices, on_device(): res.append(lax.ppermute(res[-1], axis_name='tp', perm=buffers))  18 us
    all_to_all x1, starting transfers between devices, on_device(): lax.all_to_all(my_columns, 'ep', split_axis=0, concat_axis=1, tiled=True)  16.7 us
    ppermute x8, starting transfers between devices, on_device(): res.append(lax.ppermute(res[-1], axis_name='tp', perm=buffers))  16.7 us
    all_to_all x1, starting transfers between devices, on_device(): lax.all_to_all(expert_result, 'ep', split_axis=1, concat_axis=0, tiled=True)  13.2 us
    transpose x3, local copies, waits for them, and re-layouts, laid_out(): tiles = jnp.moveaxis(tiles, 0, dim)  12.2 us
  transfers between devices with their start and end apart: 20, of which 12 were waited for; matrix products, arithmetic and copies ran while one was open for 19% of the time, Pallas kernels for 0%

profile of v1, /device:TPU:1, one launch (start us, length us, event | category | flops | bytes accessed | tf_op | source)
XLA Modules:
  0.0 359.4 jit_solution(10096136277656162502)
XLA Ops:
  7.2 1.6 fusion.4
  13.6 16.7 %all-to-all-start = ((bf16[64,24,128]{2,1,0:T(8,128)(2,1)}), bf16[64,24,128]{2,1,0:T(8,128)(2,1)S(1)}, u32[]{:S(2)}, u32[]{:S(2)}) async-start(bf16[64,24,128]{2,1,0:T(8,128)(2,1)} %bitcast.34), calls=%async_computation | async-start | bytes 786432 | tf_op jit(solution)/shard_map/all_to_all | solution.py:202
  32.7 3.5 collective-permute-start
  41.9 5.7 %collective-permute-done = bf16[3,512]{0,1:T(8,128)(2,1)S(1)} collective-permute-done((bf16[3,512]{0,1:T(8,128)(2,1)S(1)}, bf16[3,512]{0,1:T(8,128)(2,1)S(1)}, u32[]{:S(2)}, u32[]{:S(2)}) %collective-permute-start) | collective-permute-done | bytes 3104 | tf_op jit(solution)/shard_map/ppermute | solution.py:19
  52.6 5.4 %all-to-all-done = bf16[64,24,128]{2,1,0:T(8,128)(2,1)S(1)} async-done(((bf16[64,24,128]{2,1,0:T(8,128)(2,1)}), bf16[64,24,128]{2,1,0:T(8,128)(2,1)S(1)}, u32[]{:S(2)}, u32[]{:S(2)}) %all-to-all-start) | async-done | bytes 393248 | tf_op jit(solution)/shard_map/all_to_all | solution.py:202
  58.1 3.1 collective-permute-start.1
  61.2 5.6 %collective-permute-start.9 = (bf16[2,768,128]{2,1,0:T(8,128)(2,1)S(1)}, bf16[2,768,128]{2,1,0:T(8,128)(2,1)S(1)}, u32[]{:S(2)}, u32[]{:S(2)}) collective-permute-start(bf16[2,768,128]{2,1,0:T(8,128)(2,1)S(1)} %bitcast.132), channel_id=1, source_target_pairs={{0,15},{1,0},{2,1},{3,2},{4,3},{5,4},{6,5},{7,6},{8,7},{9,8},{10,9... | collective-permute-start | bytes 1179656 | tf_op jit(solution)/shard_map/ppermute | solution.py:210
  66.9 6.4 %collective-permute-done.1 = bf16[2,768,128]{2,1,0:T(8,128)(2,1)S(1)} collective-permute-done((bf16[2,768,128]{2,1,0:T(8,128)(2,1)S(1)}, bf16[2,768,128]{2,1,0:T(8,128)(2,1)S(1)}, u32[]{:S(2)}, u32[]{:S(2)}) %collective-permute-start.1) | collective-permute-done | bytes 393248 | tf_op jit(solution)/shard_map/ppermute | solution.py:208
  73.3 1.9 collective-permute-start.2
  75.2 6.7 %collective-permute-start.10 = (bf16[2,768,128]{2,1,0:T(8,128)(2,1)S(1)}, bf16[2,768,128]{2,1,0:T(8,128)(2,1)}, u32[]{:S(2)}, u32[]{:S(2)}) collective-permute-start(bf16[2,768,128]{2,1,0:T(8,128)(2,1)S(1)} %collective-permute-done.9), channel_id=1, source_target_pairs={{0,15},{1,0},{2,1},{3,2},{4,3},{5,4},{6,5},{7,6},{8,7},{9,8},{10,9... | collective-permute-start | bytes 1179656 | tf_op jit(solution)/shard_map/ppermute | solution.py:210
  81.9 5.7 %collective-permute-done.2 = bf16[2,768,128]{2,1,0:T(8,128)(2,1)} collective-permute-done((bf16[2,768,128]{2,1,0:T(8,128)(2,1)S(1)}, bf16[2,768,128]{2,1,0:T(8,128)(2,1)}, u32[]{:S(2)}, u32[]{:S(2)}) %collective-permute-start.2) | collective-permute-done | bytes 393248 | tf_op jit(solution)/shard_map/ppermute | solution.py:208
  87.6 1.9 collective-permute-start.3
  90.2 6.7 %collective-permute-start.11 = (bf16[2,768,128]{2,1,0:T(8,128)(2,1)}, bf16[2,768,128]{2,1,0:T(8,128)(2,1)}, u32[]{:S(2)}, u32[]{:S(2)}) collective-permute-start(bf16[2,768,128]{2,1,0:T(8,128)(2,1)} %collective-permute-done.10), channel_id=1, source_target_pairs={{0,15},{1,0},{2,1},{3,2},{4,3},{5,4},{6,5},{7,6},{8,7},{9,8},{10,9... | collective-permute-start | bytes 1179656 | tf_op jit(solution)/shard_map/ppermute | solution.py:210
  96.8 4.4 %collective-permute-done.3 = bf16[2,768,128]{2,1,0:T(8,128)(2,1)} collective-permute-done((bf16[2,768,128]{2,1,0:T(8,128)(2,1)}, bf16[2,768,128]{2,1,0:T(8,128)(2,1)}, u32[]{:S(2)}, u32[]{:S(2)}) %collective-permute-start.3) | collective-permute-done | bytes 393248 | tf_op jit(solution)/shard_map/ppermute | solution.py:208
  101.3 1.9 collective-permute-start.4
  104.6 2.0 fusion.12
  108.2 1.7 copy.177
  111.6 1.6 copy.168
  113.2 6.7 %collective-permute-start.12 = (bf16[2,768,128]{2,1,0:T(8,128)(2,1)}, bf16[2,768,128]{2,1,0:T(8,128)(2,1)S(1)}, u32[]{:S(2)}, u32[]{:S(2)}) collective-permute-start(bf16[2,768,128]{2,1,0:T(8,128)(2,1)} %collective-permute-done.11), channel_id=1, source_target_pairs={{0,15},{1,0},{2,1},{3,2},{4,3},{5,4},{6,5},{7,6},{8,7},{9,8},{10,9... | collective-permute-start | bytes 1179656 | tf_op jit(solution)/shard_map/ppermute | solution.py:210
  119.9 1.9 collective-permute-start.5
  123.3 1.6 collective-permute-done.12
  124.9 7.4 %collective-permute-start.13 = (bf16[2,768,128]{2,1,0:T(8,128)(2,1)S(1)}, bf16[2,768,128]{2,1,0:T(8,128)(2,1)S(1)}, u32[]{:S(2)}, u32[]{:S(2)}) collective-permute-start(bf16[2,768,128]{2,1,0:T(8,128)(2,1)S(1)} %collective-permute-done.12), channel_id=1, source_target_pairs={{0,15},{1,0},{2,1},{3,2},{4,3},{5,4},{6,5},{7,6},{8,7},{9,8},{10,9... | collective-permute-start | bytes 1179656 | tf_op jit(solution)/shard_map/ppermute | solution.py:210
  132.3 1.9 collective-permute-start.6
  137.0 7.1 %collective-permute-start.14 = (bf16[2,768,128]{2,1,0:T(8,128)(2,1)S(1)}, bf16[2,768,128]{2,1,0:T(8,128)(2,1)}, u32[]{:S(2)}, u32[]{:S(2)}) collective-permute-start(bf16[2,768,128]{2,1,0:T(8,128)(2,1)S(1)} %collective-permute-done.13), channel_id=1, source_target_pairs={{0,15},{1,0},{2,1},{3,2},{4,3},{5,4},{6,5},{7,6},{8,7},{9,8},{10,9... | collective-permute-start | bytes 1179656 | tf_op jit(solution)/shard_map/ppermute | solution.py:210
  144.5 1.9 collective-permute-start.7
  147.5 1.7 fusion.79
  149.2 6.9 %collective-permute-start.15 = (bf16[2,768,128]{2,1,0:T(8,128)(2,1)}, bf16[2,768,128]{2,1,0:T(8,128)(2,1)}, u32[]{:S(2)}, u32[]{:S(2)}) collective-permute-start(bf16[2,768,128]{2,1,0:T(8,128)(2,1)} %collective-permute-done.14), channel_id=1, source_target_pairs={{0,15},{1,0},{2,1},{3,2},{4,3},{5,4},{6,5},{7,6},{8,7},{9,8},{10,9... | collective-permute-start | bytes 1179656 | tf_op jit(solution)/shard_map/ppermute | solution.py:210
  156.6 2.1 collective-permute-start.8
  160.1 3.2 multiply_reduce_fusion
  195.2 2.0 fusion.2
  197.2 2.0 multiply_convert_fusion
  200.5 75.9 %all-gather.6.cloned.1.call-done = bf16[2883584]{0:T(1024)(128)(2,1)} async-done(((bf16[180224]{0:T(1024)(128)(2,1)}), bf16[2883584]{0:T(1024)(128)(2,1)}) %all-gather.6.cloned.1.call-update) | async-done | bytes 5767184 | tf_op jit(solution)/shard_map/all_gather | solution.py:40
  276.4 5.8 %reshape.648 = bf16[16,180224]{1,0:T(8,128)(2,1)} reshape(bf16[2883584]{0:T(1024)(128)(2,1)} %all-gather.6.cloned.1.call-done) | data formatting | bytes 11534336 | tf_op jit(solution)/shard_map/all_gather | solution.py:40
  282.2 3.8 %slice.215 = bf16[16,98304]{1,0:T(8,128)(2,1)} slice(bf16[16,180224]{1,0:T(8,128)(2,1)} %reshape.648), slice={[0:16], [65536:163840]} | slice | bytes 6291456 | tf_op jit(solution)/shard_map/slice | solution.py:42
  286.0 8.8 %reshape.642 = bf16[16,2,768,64]{3,2,1,0:T(8,128)(2,1)} reshape(bf16[16,98304]{1,0:T(8,128)(2,1)} %slice.215) | data formatting | bytes 6291456 | tf_op jit(solution)/shard_map/reshape | solution.py:42
  294.8 7.0 %copy.183 = bf16[2,768,16,64]{1,3,2,0:T(8,128)(2,1)} copy(bf16[2,768,16,64]{3,1,0,2:T(8,128)(2,1)} %bitcast.125) | data formatting | bytes 6291456 | tf_op jit(solution)/shard_map/transpose | solution.py:33
  301.8 3.3 convolution_convert_fusion.1
  306.3 13.2 %all-to-all-start.1 = ((bf16[2,768,128]{2,0,1:T(2,128)(2,1)}), bf16[2,768,128]{2,0,1:T(2,128)(2,1)S(1)}, u32[]{:S(2)}, u32[]{:S(2)}) async-start(bf16[2,768,128]{2,0,1:T(2,128)(2,1)} %copy.185), calls=%async_computation.1 | async-start | bytes 786432 | tf_op jit(solution)/shard_map/all_to_all | solution.py:232
  320.4 2.6 fusion.8
  323.0 1.9 slice.216
  324.8 1.8 copy.194
  326.7 2.8 copy.182
  329.5 3.0 reshape.645
  332.5 2.4 copy.188
  336.3 11.0 %all-to-all-done.1 = bf16[2,768,128]{2,0,1:T(2,128)(2,1)S(1)} async-done(((bf16[2,768,128]{2,0,1:T(2,128)(2,1)}), bf16[2,768,128]{2,0,1:T(2,128)(2,1)S(1)}, u32[]{:S(2)}, u32[]{:S(2)}) %all-to-all-start.1) | async-done | bytes 393248 | tf_op jit(solution)/shard_map/all_to_all | solution.py:232
  347.3 1.5 fusion.81
  348.9 1.5 convolution_add_fusion.1
  350.4 2.1 fusion.11
  (160 shorter events, 66.9 us)
Async XLA Ops:
  7.2 327.7 %copy-start = (bf16[4096,128]{1,0:T(8,128)(2,1)S(1)}, bf16[4096,128]{1,0:T(8,128)(2,1)}, u32[]{:S(2)}) copy-start(bf16[4096,128]{1,0:T(8,128)(2,1)} %param.35) | copy-start | bytes 3145732
  7.2 2.6 copy-start.11
  9.8 1.6 copy-start.7
  9.8 1.6 copy-start.9
  11.5 0.6 copy-start.5
  13.6 44.5 %all-to-all-start = ((bf16[64,24,128]{2,1,0:T(8,128)(2,1)}), bf16[64,24,128]{2,1,0:T(8,128)(2,1)S(1)}, u32[]{:S(2)}, u32[]{:S(2)}) async-start(bf16[64,24,128]{2,1,0:T(8,128)(2,1)} %bitcast.34), calls=%async_computation | async-start | bytes 786432 | tf_op jit(solution)/shard_map/all_to_all | solution.py:202
  30.3 128.4 %all-gather.4.cloned.1.call-start = ((), (), s32[]{:S(2)}) async-start(), calls=%async_computation.2 | async-start | bytes 2297856 | tf_op jit(solution)/shard_map/all_gather | solution.py:67
  32.7 15.0 %collective-permute-start = (bf16[3,512]{0,1:T(8,128)(2,1)S(1)}, bf16[3,512]{0,1:T(8,128)(2,1)S(1)}, u32[]{:S(2)}, u32[]{:S(2)}) collective-permute-start(bf16[3,512]{0,1:T(8,128)(2,1)S(1)} %copy.162), channel_id=1, source_target_pairs={{0,16},{16,32},{32,48},{48,64},{64,80},{80,96},{96,112},{112,128},... | collective-permute-start | bytes 9224 | tf_op jit(solution)/shard_map/ppermute | solution.py:19
  38.0 20.1 %copy-start.1 = (f32[2,128,4]{2,1,0:T(8,128)}, f32[2,128,4]{2,1,0:T(8,128)S(1)}, u32[]{:S(2)}) copy-start(f32[2,128,4]{2,1,0:T(8,128)S(1)} %reduce_window_sum.22) | copy-start | bytes 12292
  50.8 1.0 copy-start.2
  52.6 223.8 %all-gather.6.cloned.1.call-start = ((), (), s32[]{:S(2)}) async-start(), calls=%async_computation.3 | async-start | bytes 6127616 | tf_op jit(solution)/shard_map/all_gather | solution.py:40
  58.1 15.2 %collective-permute-start.1 = (bf16[2,768,128]{2,1,0:T(8,128)(2,1)S(1)}, bf16[2,768,128]{2,1,0:T(8,128)(2,1)S(1)}, u32[]{:S(2)}, u32[]{:S(2)}) collective-permute-start(bf16[2,768,128]{2,1,0:T(8,128)(2,1)S(1)} %bitcast.131), channel_id=1, source_target_pairs={{0,1},{1,2},{2,3},{3,4},{4,5},{5,6},{6,7},{7,8},{8,9},{9,10},{10,1... | collective-permute-start | bytes 1179656 | tf_op jit(solution)/shard_map/ppermute | solution.py:208
  61.2 14.0 %collective-permute-start.9 = (bf16[2,768,128]{2,1,0:T(8,128)(2,1)S(1)}, bf16[2,768,128]{2,1,0:T(8,128)(2,1)S(1)}, u32[]{:S(2)}, u32[]{:S(2)}) collective-permute-start(bf16[2,768,128]{2,1,0:T(8,128)(2,1)S(1)} %bitcast.132), channel_id=1, source_target_pairs={{0,15},{1,0},{2,1},{3,2},{4,3},{5,4},{6,5},{7,6},{8,7},{9,8},{10,9... | collective-permute-start | bytes 1179656 | tf_op jit(solution)/shard_map/ppermute | solution.py:210
  73.3 14.3 %collective-permute-start.2 = (bf16[2,768,128]{2,1,0:T(8,128)(2,1)S(1)}, bf16[2,768,128]{2,1,0:T(8,128)(2,1)}, u32[]{:S(2)}, u32[]{:S(2)}) collective-permute-start(bf16[2,768,128]{2,1,0:T(8,128)(2,1)S(1)} %collective-permute-done.1), channel_id=1, source_target_pairs={{0,1},{1,2},{2,3},{3,4},{4,5},{5,6},{6,7},{7,8},{8,9},{9,10},{10,1... | collective-permute-start | bytes 1179656 | tf_op jit(solution)/shard_map/ppermute | solution.py:208
  75.2 14.9 %collective-permute-start.10 = (bf16[2,768,128]{2,1,0:T(8,128)(2,1)S(1)}, bf16[2,768,128]{2,1,0:T(8,128)(2,1)}, u32[]{:S(2)}, u32[]{:S(2)}) collective-permute-start(bf16[2,768,128]{2,1,0:T(8,128)(2,1)S(1)} %collective-permute-done.9), channel_id=1, source_target_pairs={{0,15},{1,0},{2,1},{3,2},{4,3},{5,4},{6,5},{7,6},{8,7},{9,8},{10,9... | collective-permute-start | bytes 1179656 | tf_op jit(solution)/shard_map/ppermute | solution.py:210
  87.6 13.6 %collective-permute-start.3 = (bf16[2,768,128]{2,1,0:T(8,128)(2,1)}, bf16[2,768,128]{2,1,0:T(8,128)(2,1)}, u32[]{:S(2)}, u32[]{:S(2)}) collective-permute-start(bf16[2,768,128]{2,1,0:T(8,128)(2,1)} %collective-permute-done.2), channel_id=1, source_target_pairs={{0,1},{1,2},{2,3},{3,4},{4,5},{5,6},{6,7},{7,8},{8,9},{9,10},{10,1... | collective-permute-start | bytes 1179656 | tf_op jit(solution)/shard_map/ppermute | solution.py:208
  90.2 23.0 %collective-permute-start.11 = (bf16[2,768,128]{2,1,0:T(8,128)(2,1)}, bf16[2,768,128]{2,1,0:T(8,128)(2,1)}, u32[]{:S(2)}, u32[]{:S(2)}) collective-permute-start(bf16[2,768,128]{2,1,0:T(8,128)(2,1)} %collective-permute-done.10), channel_id=1, source_target_pairs={{0,15},{1,0},{2,1},{3,2},{4,3},{5,4},{6,5},{7,6},{8,7},{9,8},{10,9... | collective-permute-start | bytes 1179656 | tf_op jit(solution)/shard_map/ppermute | solution.py:210
  101.3 18.6 %collective-permute-start.4 = (bf16[2,768,128]{2,1,0:T(8,128)(2,1)}, bf16[2,768,128]{2,1,0:T(8,128)(2,1)}, u32[]{:S(2)}, u32[]{:S(2)}) collective-permute-start(bf16[2,768,128]{2,1,0:T(8,128)(2,1)} %collective-permute-done.3), channel_id=1, source_target_pairs={{0,1},{1,2},{2,3},{3,4},{4,5},{5,6},{6,7},{7,8},{8,9},{9,10},{10,1... | collective-permute-start | bytes 1179656 | tf_op jit(solution)/shard_map/ppermute | solution.py:208
  113.2 11.7 %collective-permute-start.12 = (bf16[2,768,128]{2,1,0:T(8,128)(2,1)}, bf16[2,768,128]{2,1,0:T(8,128)(2,1)S(1)}, u32[]{:S(2)}, u32[]{:S(2)}) collective-permute-start(bf16[2,768,128]{2,1,0:T(8,128)(2,1)} %collective-permute-done.11), channel_id=1, source_target_pairs={{0,15},{1,0},{2,1},{3,2},{4,3},{5,4},{6,5},{7,6},{8,7},{9,8},{10,9... | collective-permute-start | bytes 1179656 | tf_op jit(solution)/shard_map/ppermute | solution.py:210
  119.9 12.4 %collective-permute-start.5 = (bf16[2,768,128]{2,1,0:T(8,128)(2,1)}, bf16[2,768,128]{2,1,0:T(8,128)(2,1)}, u32[]{:S(2)}, u32[]{:S(2)}) collective-permute-start(bf16[2,768,128]{2,1,0:T(8,128)(2,1)} %collective-permute-done.4), channel_id=1, source_target_pairs={{0,1},{1,2},{2,3},{3,4},{4,5},{5,6},{6,7},{7,8},{8,9},{9,10},{10,1... | collective-permute-start | bytes 1179656 | tf_op jit(solution)/shard_map/ppermute | solution.py:208
  124.9 12.1 %collective-permute-start.13 = (bf16[2,768,128]{2,1,0:T(8,128)(2,1)S(1)}, bf16[2,768,128]{2,1,0:T(8,128)(2,1)S(1)}, u32[]{:S(2)}, u32[]{:S(2)}) collective-permute-start(bf16[2,768,128]{2,1,0:T(8,128)(2,1)S(1)} %collective-permute-done.12), channel_id=1, source_target_pairs={{0,15},{1,0},{2,1},{3,2},{4,3},{5,4},{6,5},{7,6},{8,7},{9,8},{10,9... | collective-permute-start | bytes 1179656 | tf_op jit(solution)/shard_map/ppermute | solution.py:210
  132.3 12.2 %collective-permute-start.6 = (bf16[2,768,128]{2,1,0:T(8,128)(2,1)}, bf16[2,768,128]{2,1,0:T(8,128)(2,1)}, u32[]{:S(2)}, u32[]{:S(2)}) collective-permute-start(bf16[2,768,128]{2,1,0:T(8,128)(2,1)} %collective-permute-done.5), channel_id=1, source_target_pairs={{0,1},{1,2},{2,3},{3,4},{4,5},{5,6},{6,7},{7,8},{8,9},{9,10},{10,1... | collective-permute-start | bytes 1179656 | tf_op jit(solution)/shard_map/ppermute | solution.py:208
  137.0 12.2 %collective-permute-start.14 = (bf16[2,768,128]{2,1,0:T(8,128)(2,1)S(1)}, bf16[2,768,128]{2,1,0:T(8,128)(2,1)}, u32[]{:S(2)}, u32[]{:S(2)}) collective-permute-start(bf16[2,768,128]{2,1,0:T(8,128)(2,1)S(1)} %collective-permute-done.13), channel_id=1, source_target_pairs={{0,15},{1,0},{2,1},{3,2},{4,3},{5,4},{6,5},{7,6},{8,7},{9,8},{10,9... | collective-permute-start | bytes 1179656 | tf_op jit(solution)/shard_map/ppermute | solution.py:210
  144.5 12.1 %collective-permute-start.7 = (bf16[2,768,128]{2,1,0:T(8,128)(2,1)}, bf16[2,768,128]{2,1,0:T(8,128)(2,1)}, u32[]{:S(2)}, u32[]{:S(2)}) collective-permute-start(bf16[2,768,128]{2,1,0:T(8,128)(2,1)} %collective-permute-done.6), channel_id=1, source_target_pairs={{0,1},{1,2},{2,3},{3,4},{4,5},{5,6},{6,7},{7,8},{8,9},{9,10},{10,1... | collective-permute-start | bytes 1179656 | tf_op jit(solution)/shard_map/ppermute | solution.py:208
  149.2 31.7 %collective-permute-start.15 = (bf16[2,768,128]{2,1,0:T(8,128)(2,1)}, bf16[2,768,128]{2,1,0:T(8,128)(2,1)}, u32[]{:S(2)}, u32[]{:S(2)}) collective-permute-start(bf16[2,768,128]{2,1,0:T(8,128)(2,1)} %collective-permute-done.14), channel_id=1, source_target_pairs={{0,15},{1,0},{2,1},{3,2},{4,3},{5,4},{6,5},{7,6},{8,7},{9,8},{10,9... | collective-permute-start | bytes 1179656 | tf_op jit(solution)/shard_map/ppermute | solution.py:210
  156.6 12.1 %collective-permute-start.8 = (bf16[2,768,128]{2,1,0:T(8,128)(2,1)}, bf16[2,768,128]{2,1,0:T(8,128)(2,1)}, u32[]{:S(2)}, u32[]{:S(2)}) collective-permute-start(bf16[2,768,128]{2,1,0:T(8,128)(2,1)} %collective-permute-done.7), channel_id=1, source_target_pairs={{0,1},{1,2},{2,3},{3,4},{4,5},{5,6},{6,7},{7,8},{8,9},{9,10},{10,1... | collective-permute-start | bytes 1179656 | tf_op jit(solution)/shard_map/ppermute | solution.py:208
  168.2 27.0 %copy-start.3 = (bf16[2,2048,64]{1,2,0:T(8,128)(2,1)S(1)}, bf16[2,2048,64]{1,2,0:T(8,128)(2,1)}, u32[]{:S(2)}) copy-start(bf16[2,2048,64]{1,2,0:T(8,128)(2,1)} %param.40) | copy-start | bytes 1572868
  177.0 20.3 %copy-start.4 = (bf16[2,2048,64]{1,2,0:T(8,128)(2,1)S(1)}, bf16[2,2048,64]{1,2,0:T(8,128)(2,1)}, u32[]{:S(2)}) copy-start(bf16[2,2048,64]{1,2,0:T(8,128)(2,1)} %param.41) | copy-start | bytes 1572868
  186.5 13.2 %copy-start.6 = (bf16[16384]{0:T(1024)(128)(2,1)S(1)}, bf16[16384]{0:T(1024)(128)(2,1)}, u32[]{:S(2)}) copy-start(bf16[16384]{0:T(1024)(128)(2,1)} %reshape.639) | copy-start | bytes 98308
  286.0 34.4 %copy-start.8 = (s32[1,256]{1,0:T(1,128)S(1)}, s32[1,256]{1,0:T(1,128)}, u32[]{:S(2)}) copy-start(s32[1,256]{1,0:T(1,128)} %copy-done.7) | copy-start | bytes 3076
  286.0 34.4 %copy-start.10 = (s32[1,256]{1,0:T(1,128)S(1)}, s32[1,256]{1,0:T(1,128)}, u32[]{:S(2)}) copy-start(s32[1,256]{1,0:T(1,128)} %copy-done.9) | copy-start | bytes 3076
  294.8 30.0 %slice-start = ((bf16[16,180224]{1,0:T(8,128)(2,1)}), bf16[16,65536]{1,0:T(8,128)(2,1)S(1)}, s32[]{:S(2)}) async-start(bf16[16,180224]{1,0:T(8,128)(2,1)} %reshape.648), calls=%async_computation.4 | async-start | bytes 4194304 | tf_op jit(solution)/shard_map/slice | solution.py:42
  306.3 40.9 %all-to-all-start.1 = ((bf16[2,768,128]{2,0,1:T(2,128)(2,1)}), bf16[2,768,128]{2,0,1:T(2,128)(2,1)S(1)}, u32[]{:S(2)}, u32[]{:S(2)}) async-start(bf16[2,768,128]{2,0,1:T(2,128)(2,1)} %copy.185), calls=%async_computation.1 | async-start | bytes 786432 | tf_op jit(solution)/shard_map/all_to_all | solution.py:232
Sparse Core Ops, SparseCore 0:
  52.7 75.2 all-gather.3
  200.6 75.7 all-gather.5
